TPU v7x, 32 devices: a whole 2x2x4 slice. The times are simulated.
32 devices in a mesh: sp: 8 (over z, y), tp: 4 (over x, core).
Axes of the slice: x: 2, y: 2, z: 4, core: 2. Of those that a mesh axis runs over, the one named last changes fastest.
Arguments:
- tokens: bfloat16 [3072, 2048], P(('sp', 'tp')), may hold values from -60 to 60
- query_weight: bfloat16 [2048, 1024], P(None, 'tp'), may hold values from -0.125 to 0.125
- key_weight: bfloat16 [2048, 1024], P(None, 'tp'), may hold values from -0.125 to 0.125
- value_weight: bfloat16 [2048, 1024], P(None, 'tp'), may hold values from -0.125 to 0.125
- outer_gate: bfloat16 [2048, 1024], P(None, 'tp'), may hold values from -0.125 to 0.125
- inner_gate: bfloat16 [2048, 1024], P(None, 'tp'), may hold values from -0.125 to 0.125
- conv_weight: bfloat16 [2048, 1024], P(None, 'tp'), may hold values from -0.125 to 0.125
- conv_taps: bfloat16 [3, 1024], P(None, 'tp'), may hold values from -3 to 3
- gate_sum: float32 [8, 3072], P('tp'), may hold values from -180 to 0, as said below
- head_gain: bfloat16 [1024], P('tp'), may hold values from 0.099609375 to 1.8984375
- channel_gain: bfloat16 [1024], P('tp'), may hold values from 0.099609375 to 1.8984375
- attention_out: bfloat16 [1024, 2048], P('tp'), may hold values from -0.125 to 0.125
- channel_out: bfloat16 [1024, 2048], P('tp'), may hold values from -0.125 to 0.125
Outputs:
- mixed_out: bfloat16 [3072, 2048], P(('sp', 'tp'))
Inputs may be any that keep to these rules, and one draw needn't show every extreme that they name: gate_sum[h, t] never rises with t.
All inputs are finite; a program needn't handle non-finite values.
Results may differ from a plain program's by a relative error of at most 0.015.
Values may be sent and summed in bfloat16 or wider, within the bound.
A program may use at most 192 MiB of HBM per device.

v0:
```python
import jax
import jax.numpy as jnp
from jax import lax
from jax.sharding import PartitionSpec as P

HEAD = 128
KTAP = 3


def passed_along(shard, axis, by):
    peers = lax.axis_size(axis)
    pairs = [(i, i + by) for i in range(peers) if 0 <= i + by < peers]
    return lax.ppermute(shard, axis, pairs)


def head_norm(values, gain_vector):
    row_count = values.shape[0]
    shaped = values.reshape(row_count, -1, HEAD)
    shaped = shaped * lax.rsqrt(jnp.mean(shaped * shaped, axis=-1, keepdims=True) + 1e-06)
    return (shaped.reshape(row_count, -1) * gain_vector.astype(jnp.float32)).astype(jnp.bfloat16)


def block_size(total_rows, unit_rows):
    best_rows = unit_rows
    for factor in range(1, total_rows // unit_rows + 1):
        if total_rows // unit_rows % factor == 0 and factor * unit_rows <= 2048:
            best_rows = factor * unit_rows
    return best_rows


def local(
    tokens,
    query_weight,
    key_weight,
    value_weight,
    outer_gate,
    inner_gate,
    conv_weight,
    conv_taps,
    gate_sum,
    head_gain,
    channel_gain,
    attention_out,
    channel_out,
):
    weight_list = (query_weight, key_weight, value_weight, outer_gate, inner_gate, conv_weight)

    def project_rows(piece_rows):
        return jnp.concatenate(
            [
                jnp.dot(piece_rows, weight, preferred_element_type=jnp.float32).astype(jnp.bfloat16)
                for weight in weight_list
            ],
            axis=1,
        )

    projected = project_rows(lax.all_gather(tokens, "tp", axis=0, tiled=True))
    pieces_list = []
    offset = 0
    for weight in weight_list:
        pieces_list.append(projected[:, offset : offset + weight.shape[1]])
        offset = offset + weight.shape[1]
    queries, keys_here, values_here, gate_outer, gate_inner, conv_input = pieces_list
    row_count = projected.shape[0]
    first_row = lax.axis_index("sp") * row_count
    mixed_in = (gate_inner.astype(jnp.float32) * conv_input.astype(jnp.float32)).astype(
        jnp.bfloat16
    )
    carried = passed_along(mixed_in[row_count - (KTAP - 1) :], "sp", 1)
    padded = jnp.concatenate([carried, mixed_in], axis=0).astype(jnp.float32)
    summed = jnp.zeros(mixed_in.shape, jnp.float32)
    for offset in range(KTAP):
        summed = (
            summed + conv_taps[offset].astype(jnp.float32) * padded[offset : offset + row_count]
        )
    conv_out = gate_outer.astype(jnp.float32) * summed
    heads_here = queries.shape[1] // HEAD
    query_heads = queries.reshape(row_count, heads_here, HEAD)
    query_gate = lax.dynamic_slice_in_dim(gate_sum, first_row, row_count, 1).T
    query_pos = first_row + jnp.arange(row_count, dtype=jnp.int32)
    last_row = first_row + row_count - 1
    score_scale = HEAD ** (-0.5)
    initial = (
        jnp.full((row_count, heads_here), -jnp.inf, jnp.float32),
        jnp.zeros((row_count, heads_here), jnp.float32),
        jnp.zeros((row_count, heads_here, HEAD), jnp.float32),
    )
    key_piece = lax.all_gather(keys_here, "sp", axis=0, tiled=True)
    value_piece = lax.all_gather(values_here, "sp", axis=0, tiled=True)
    piece_length = key_piece.shape[0]
    span_rows = block_size(piece_length, row_count)

    def one_block(block_index, state_in):
        key_start = block_index * span_rows

        def work(state_old):
            peak_old, total_old, accum_old = state_old
            key_block = lax.dynamic_slice_in_dim(
                key_piece, block_index * span_rows, span_rows, 0
            ).reshape(span_rows, heads_here, HEAD)
            value_block = lax.dynamic_slice_in_dim(
                value_piece, block_index * span_rows, span_rows, 0
            ).reshape(span_rows, heads_here, HEAD)
            gate_block = lax.dynamic_slice_in_dim(gate_sum, key_start, span_rows, 1)
            logits = (
                jnp.einsum(
                    "qhd,khd->qhk", query_heads, key_block, preferred_element_type=jnp.float32
                )
                * score_scale
            )
            logits = logits + query_gate[:, :, None] - gate_block[None, :, :]
            key_pos = key_start + jnp.arange(span_rows, dtype=jnp.int32)
            allowed = (key_pos[None, :] <= query_pos[:, None])[:, None, :]
            peak_new = jnp.maximum(peak_old, jnp.max(jnp.where(allowed, logits, -jnp.inf), axis=-1))
            peak_safe = jnp.where(peak_new > -jnp.inf, peak_new, 0.0)
            weights = jnp.where(allowed, jnp.exp(logits - peak_safe[..., None]), 0.0)
            rescale = jnp.exp(peak_old - peak_safe)
            total_new = total_old * rescale + jnp.sum(weights, axis=-1)
            accum_new = accum_old * rescale[..., None] + jnp.einsum(
                "qhk,khd->qhd",
                weights.astype(jnp.bfloat16),
                value_block,
                preferred_element_type=jnp.float32,
            )
            return (peak_new, total_new, accum_new)

        return lax.cond(key_start <= last_row, work, lambda state_old: state_old, state_in)

    peak_end, total_end, accum_end = lax.fori_loop(0, piece_length // span_rows, one_block, initial)
    attention = (accum_end / total_end[..., None]).reshape(row_count, heads_here * HEAD)
    head_normed = head_norm(attention, head_gain)
    group_normed = head_norm(conv_out, channel_gain)
    return lax.psum_scatter(
        (
            jnp.dot(head_normed, attention_out, preferred_element_type=jnp.float32)
            + jnp.dot(group_normed, channel_out, preferred_element_type=jnp.float32)
        ).astype(jnp.bfloat16),
        "tp",
        scatter_dimension=0,
        tiled=True,
    )


def solution(mesh):
    placed = (
        P(("sp", "tp"), None),
        P(None, "tp"),
        P(None, "tp"),
        P(None, "tp"),
        P(None, "tp"),
        P(None, "tp"),
        P(None, "tp"),
        P(None, "tp"),
        P("tp", None),
        P("tp"),
        P("tp"),
        P("tp", None),
        P("tp", None),
    )
    return jax.shard_map(
        local, mesh=mesh, in_specs=placed, out_specs=P(("sp", "tp"), None), check_vma=False
    )
```

profile of v0, /device:TPU:0, one launch (start us, length us, event | category | flops | bytes accessed | tf_op | source)
XLA Modules:
  0.0 174.2 jit_solution(3127703102989891153)
XLA Ops:
  6.5 0.7 all-gather.4.cloned.1.call-update
  7.3 24.0 %all-gather.4.cloned.1.call-done = bf16[384,2048]{1,0:T(8,128)(2,1)} async-done(((bf16[96,2048]{1,0:T(8,128)(2,1)}), bf16[384,2048]{1,0:T(8,128)(2,1)}) %all-gather.4.cloned.1.call-update) | async-done | bytes 1572880 | tf_op jit(solution)/shard_map/all_gather | solution.py:57
  31.3 3.1 %convolution_convert_fusion.3 = bf16[384,256]{1,0:T(8,128)(2,1)} fusion(bf16[384,2048]{1,0:T(8,128)(2,1)} %all-gather.4.cloned.1.call-done, bf16[2048,256]{1,0:T(8,128)(2,1)} %param.20), kind=kOutput, calls=%fused_computation.32 | convolution fusion | flops 402751488 | bytes 2818048 | tf_op jit(solution)/shard_map/dot_general | solution.py:51
  34.5 2.5 %convolution_convert_fusion.5 = bf16[384,256]{1,0:T(8,128)(2,1)} fusion(bf16[384,2048]{1,0:T(8,128)(2,1)S(1)} %copy-done.1, bf16[2048,256]{1,0:T(8,128)(2,1)} %param.19), kind=kOutput, calls=%fused_computation.34 | convolution fusion | flops 402751488 | bytes 2818048 | tf_op jit(solution)/shard_map/dot_general | solution.py:51
  37.1 2.1 %fusion.19 = f32[384,256]{0,1:T(8,128)S(1)} fusion(bf16[384,2048]{1,0:T(8,128)(2,1)S(1)} %copy-done.1, bf16[2048,256]{1,0:T(8,128)(2,1)} %param.22), kind=kOutput, calls=%fused_computation.28 | convolution fusion | flops 402849792 | bytes 3014656 | tf_op jit(solution)/shard_map/dot_general | solution.py:51
  39.2 0.8 fusion.22
  40.1 3.4 %collective-permute-start = (bf16[2,256]{0,1:T(8,128)(2,1)S(1)}, bf16[2,256]{0,1:T(8,128)(2,1)S(1)}, u32[]{:S(2)}, u32[]{:S(2)}) collective-permute-start(bf16[2,256]{0,1:T(8,128)(2,1)S(1)} %slice.28), channel_id=1, source_target_pairs={{0,4},{4,8},{8,12},{12,16},{16,20},{20,24},{24,28},{1,5},{5,9},{9,... | collective-permute-start | bytes 3080 | tf_op jit(solution)/shard_map/ppermute | solution.py:13
  43.5 0.8 convolution_convert_fusion.4
  44.4 2.1 %collective-permute-done = bf16[2,256]{0,1:T(8,128)(2,1)S(1)} collective-permute-done((bf16[2,256]{0,1:T(8,128)(2,1)S(1)}, bf16[2,256]{0,1:T(8,128)(2,1)S(1)}, u32[]{:S(2)}, u32[]{:S(2)}) %collective-permute-start) | collective-permute-done | bytes 1056 | tf_op jit(solution)/shard_map/ppermute | solution.py:13
  46.7 2.0 %bitcast_reduce_fusion = (f32[384,2]{0,1:T(2,128)S(1)}, f32[384,256]{0,1:T(8,128)S(1)}) fusion(f32[386,256]{0,1:T(8,128)S(1)} %maximum_convert_fusion, f32[256]{0:T(256)S(1)} %bitcast.51, f32[256]{0:T(256)S(1)} %bitcast.52, f32[256]{0:T(256)S(1)} %bitcast.50, bf16[384,2048]{1,0:T(8,128)(2,1)S(1)} %copy-done.1, bf16[2048,256]{1,0:T(8,128)(2,1)} %param.21), kind=kOutput, calls=%fused_computation.44 | convolution fusion | flops 403635456 | bytes 4200448 | tf_op jit(solution)/shard_map/dot_general | solution.py:51
  48.8 30.6 %all-gather.8.cloned.1.call-done = bf16[3072,256]{1,0:T(8,128)(2,1)} async-done(((bf16[384,256]{1,0:T(8,128)(2,1)}), bf16[3072,256]{1,0:T(8,128)(2,1)}) %all-gather.8.cloned.1.call-update) | async-done | bytes 1572880 | tf_op jit(solution)/shard_map/all_gather | solution.py:89
  79.4 1.7 copy.23
  81.1 43.0 %all-gather.6.cloned.1.call-done = bf16[3072,256]{1,0:T(8,128)(2,1)} async-done(((bf16[384,256]{1,0:T(8,128)(2,1)}), bf16[3072,256]{1,0:T(8,128)(2,1)}) %all-gather.6.cloned.1.call-update) | async-done | bytes 1572880 | tf_op jit(solution)/shard_map/all_gather | solution.py:88
  124.2 2.6 %copy.21 = bf16[3072,256]{0,1:T(8,128)(2,1)} copy(bf16[3072,256]{1,0:T(8,128)(2,1)} %all-gather.6.cloned.1.call-done) | data formatting | bytes 3145728
  126.8 5.5 %while.18 = (s32[]{:T(128)}, f32[384,2]{0,1:T(2,128)S(1)}, f32[384,2]{0,1:T(2,128)S(1)}, f32[384,2,128]{0,2,1:T(8,128)S(1)}, s32[]{:T(128)}, /*index=5*/bf16[307...) while((s32[]{:T(128)}, f32[384,2]{0,1:T(2,128)S(1)}, ...), condition=%wide.region_5.6_spmd.clone, body=%wide.region_0.5_spmd.clone.sunk | while | flops 617748864 | bytes 22327704 | solution.py:129
  126.9 5.4 %conditional.3 = ((f32[384,2]{0,1:T(2,128)S(1)}, f32[384,2]{0,1:T(2,128)S(1)}, f32[384,2,128]{0,2,1:T(8,128)S(1)})) conditional(s32[]{:T(128)} %convert_element_type.120, (f32[384,2]{0,1:T(2,128)S(1)}, f32[384,2]{0,1:T(2,128)S(1)}, f32[384,2,128]{0,2,1:T(8,128)S(1)}) %tuple.51, (s32[]{:T(128)}, s32[]{:T(128)}, s32[]{:T(128)}, ...), branch_computations={%region_1.0_spmd, %region_2.4_spmd} | conditional | flops 617748864 | bytes 22325888 | solution.py:127
  127.3 1.2 constant_dynamic-slice_fusion
  128.6 1.5 select_reduce_fusion
  130.1 0.9 fusion.4
  131.1 1.2 fusion.13
  132.6 0.6 fusion.28
  133.2 0.6 copy-done.4
  133.9 1.8 %add_convert_fusion = bf16[384,2048]{1,0:T(8,128)(2,1)} fusion(f32[384,2048]{1,0:T(8,128)S(1)} %fusion.28, bf16[384,256]{0,1:T(8,128)(2,1)S(1)} %fusion.26, bf16[256,2048]{1,0:T(8,128)(2,1)S(1)} %copy-done.4), kind=kOutput, calls=%fused_computation.23 | convolution fusion | flops 404226048 | bytes 5963776 | tf_op jit(solution)/shard_map/dot_general | solution.py:136
  135.7 32.0 %reduce-scatter.2.cloned.1.call-done = bf16[96,2048]{1,0:T(8,128)(2,1)} async-done(((bf16[384,2048]{1,0:T(8,128)(2,1)}), bf16[96,2048]{1,0:T(8,128)(2,1)}) %reduce-scatter.2.cloned.1.call-update) | async-done | bytes 393232 | tf_op jit(solution)/shard_map/reduce_scatter | solution.py:133
  (50 shorter events, 1.4 us)
Async XLA Ops:
  6.5 126.1 %copy-start = (bf16[256,2048]{1,0:T(8,128)(2,1)S(1)}, bf16[256,2048]{1,0:T(8,128)(2,1)}, u32[]{:S(2)}) copy-start(bf16[256,2048]{1,0:T(8,128)(2,1)} %param.28) | copy-start | bytes 3145732
  6.5 24.7 %all-gather.4.cloned.1.call-start = ((), (), s32[]{:S(2)}) async-start(), calls=%async_computation.1 | async-start | bytes 1966080 | tf_op jit(solution)/shard_map/all_gather | solution.py:57
  7.3 72.2 %all-gather.8.cloned.1.call-start = ((), (), s32[]{:S(2)}) async-start(), calls=%async_computation.3 | async-start | bytes 1769472 | tf_op jit(solution)/shard_map/all_gather | solution.py:89
  31.3 3.2 %copy-start.1 = (bf16[384,2048]{1,0:T(8,128)(2,1)S(1)}, bf16[384,2048]{1,0:T(8,128)(2,1)}, u32[]{:S(2)}) copy-start(bf16[384,2048]{1,0:T(8,128)(2,1)} %all-gather.4.cloned.1.call-done) | copy-start | bytes 4718596
  34.4 2.7 %copy-start.7 = (bf16[256]{0:T(256)(128)(2,1)S(1)}, bf16[256]{0:T(256)(128)(2,1)}, u32[]{:S(2)}) copy-start(bf16[256]{0:T(256)(128)(2,1)} %param.26) | copy-start | bytes 1540
  34.4 2.7 %copy-start.8 = (bf16[256]{0:T(256)(128)(2,1)S(1)}, bf16[256]{0:T(256)(128)(2,1)}, u32[]{:S(2)}) copy-start(bf16[256]{0:T(256)(128)(2,1)} %param.27) | copy-start | bytes 1540
  34.4 2.7 %copy-start.5 = (f32[2,3072]{1,0:T(2,128)S(1)}, f32[2,3072]{1,0:T(2,128)}, u32[]{:S(2)}) copy-start(f32[2,3072]{1,0:T(2,128)} %param.25) | copy-start | bytes 73732
  34.4 2.7 %copy-start.6 = (bf16[3,256]{1,0:T(4,128)(2,1)S(1)}, bf16[3,256]{1,0:T(4,128)(2,1)}, u32[]{:S(2)}) copy-start(bf16[3,256]{1,0:T(4,128)(2,1)} %param.24) | copy-start | bytes 4612
  34.4 89.8 %all-gather.6.cloned.1.call-start = ((), (), s32[]{:S(2)}) async-start(), calls=%async_computation.2 | async-start | bytes 1769472 | tf_op jit(solution)/shard_map/all_gather | solution.py:88
  37.0 130.7 %reduce-scatter.2.cloned.1.call-start = ((), (), s32[]{:S(2)}) async-start(), calls=%async_computation.4 | async-start | bytes 1966080 | tf_op jit(solution)/shard_map/reduce_scatter | solution.py:133
  37.1 2.1 %copy-start.2 = (bf16[2048,256]{1,0:T(8,128)(2,1)S(1)}, bf16[2048,256]{1,0:T(8,128)(2,1)}, u32[]{:S(2)}) copy-start(bf16[2048,256]{1,0:T(8,128)(2,1)} %param.23) | copy-start | bytes 3145732
  39.2 4.3 %copy-start.3 = (bf16[2048,256]{1,0:T(8,128)(2,1)S(1)}, bf16[2048,256]{1,0:T(8,128)(2,1)}, u32[]{:S(2)}) copy-start(bf16[2048,256]{1,0:T(8,128)(2,1)} %param.18) | copy-start | bytes 3145732
  40.1 6.5 %collective-permute-start = (bf16[2,256]{0,1:T(8,128)(2,1)S(1)}, bf16[2,256]{0,1:T(8,128)(2,1)S(1)}, u32[]{:S(2)}, u32[]{:S(2)}) collective-permute-start(bf16[2,256]{0,1:T(8,128)(2,1)S(1)} %slice.28), channel_id=1, source_target_pairs={{0,4},{4,8},{8,12},{12,16},{16,20},{20,24},{24,28},{1,5},{5,9},{9,... | collective-permute-start | bytes 3080 | tf_op jit(solution)/shard_map/ppermute | solution.py:13
  132.6 1.2 copy-start.4
Sparse Core Ops, SparseCore 0:
  8.9 22.3 all-gather.3
  34.5 44.8 all-gather.7
  81.6 42.5 all-gather.5
  135.8 31.8 reduce-scatter.1
where the time goes:
time: 175 us; the launch traced here: 174 us
  waiting for transfers between devices  133 us (76%)
  matrix products  16.3 us (9%)
  between operations  13.4 us (8%)
  local copies, waits for them, and re-layouts  6.53 us (4%)
  starting transfers between devices  3.5 us (2%)
  other arithmetic  1.84 us (1%)
    all_gather x1, waiting for transfers between devices, local(): key_piece = lax.all_gather(keys_here, 'sp', axis=0, tiled=True)  43 us
    reduce_scatter x1, waiting for transfers between devices, local(): lax.psum_scatter((jnp.dot(head_normed, attention_out, preferred_element_t...  32 us
    all_gather x1, waiting for transfers between devices, local(): value_piece = lax.all_gather(values_here, 'sp', axis=0, tiled=True)  30.6 us
    all_gather x1, waiting for transfers between devices, local(): projected = project_rows(lax.all_gather(tokens, 'tp', axis=0, tiled=True))  24 us
    dot_general x6, matrix products, project_rows(): jnp.dot(piece_rows, weight, preferred_element_type=jnp.float32)  11.2 us
    unnamed x21, local copies, waits for them, and re-layouts  5.14 us
  transfers between devices with their start and end apart: 5, of which 5 were waited for; matrix products, arithmetic and copies ran while one was open for 6% of the time, Pallas kernels for 0%

commit v1 on v0

--- a/solution.py
+++ b/solution.py
@@ -86,7 +86,12 @@
         jnp.zeros((row_count, heads_here, HEAD), jnp.float32),
     )
     key_piece = lax.all_gather(keys_here, "sp", axis=0, tiled=True)
-    value_piece = lax.all_gather(values_here, "sp", axis=0, tiled=True)
+    ring = [values_here]
+    for hop in range(7):
+        ring.append(lax.ppermute(ring[-1], "sp", [(dev, (dev + 1) % 8) for dev in range(8)]))
+    value_piece = jnp.roll(
+        jnp.concatenate(ring[::-1], axis=0), (lax.axis_index("sp") + 1) * ring[0].shape[0], axis=0
+    )
     piece_length = key_piece.shape[0]
     span_rows = block_size(piece_length, row_count)
 

time: 175 us -> 169 us (0.966)
  waiting for transfers between devices: 133 us -> 120 us
  local copies, waits for them, and re-layouts: 6.53 us -> 14.3 us
  matrix products: 16.3 us -> 13.8 us
  other arithmetic: 1.84 us -> 3.72 us
    ppermute x0 -> x7, waiting for transfers between devices: none -> 51.8 us  [local(): lax.ppermute(ring[-1], 'sp', [(dev, (dev + 1) % 8) for dev in range(8)])]
    all_gather x1 -> x0, waiting for transfers between devices: 30.6 us -> none  [local(): value_piece = lax.all_gather(values_here, 'sp', axis=0, tiled=True)]
    all_gather x1, waiting for transfers between devices: 43 us -> 14 us  [local(): key_piece = lax.all_gather(keys_here, 'sp', axis=0, tiled=True)]
    unnamed x21 -> x46, local copies, waits for them, and re-layouts: 5.14 us -> 10.6 us
    dot_general x6, matrix products: 11.2 us -> 8.68 us  [project_rows(): jnp.dot(piece_rows, weight, preferred_element_type=jnp.float32)]
    ppermute x1, waiting for transfers between devices: 2.11 us -> 0.01 us  [passed_along(): return lax.ppermute(shard, axis, pairs)]
    ppermute x1, starting transfers between devices: 3.38 us -> 1.29 us  [passed_along(): return lax.ppermute(shard, axis, pairs)]
    all_gather x1, waiting for transfers between devices: 24 us -> 21.9 us  [local(): projected = project_rows(lax.all_gather(tokens, 'tp', axis=0, tiled=True))]
  transfers between devices with their start and end apart: 5 -> 11, of which waited for: 5 -> 10; matrix products, arithmetic and copies ran while one was open for 6% -> 11% of each run, Pallas kernels for 0% -> 0%
where the time goes in v1:
time: 169 us
  waiting for transfers between devices  120 us (71%)
  local copies, waits for them, and re-layouts  14.3 us (8%)
  matrix products  13.8 us (8%)
  between operations  13.4 us (8%)
  other arithmetic  3.72 us (2%)
  starting transfers between devices  2.92 us (2%)
    ppermute x7, waiting for transfers between devices, local(): lax.ppermute(ring[-1], 'sp', [(dev, (dev + 1) % 8) for dev in range(8)])  51.8 us
    reduce_scatter x1, waiting for transfers between devices, local(): lax.psum_scatter((jnp.dot(head_normed, attention_out, preferred_element_t...  32 us
    all_gather x1, waiting for transfers between devices, local(): projected = project_rows(lax.all_gather(tokens, 'tp', axis=0, tiled=True))  21.9 us
    all_gather x1, waiting for transfers between devices, local(): key_piece = lax.all_gather(keys_here, 'sp', axis=0, tiled=True)  14 us
    unnamed x46, local copies, waits for them, and re-layouts  10.6 us
    dot_general x6, matrix products, project_rows(): jnp.dot(piece_rows, weight, preferred_element_type=jnp.float32)  8.68 us
  transfers between devices with their start and end apart: 11, of which 10 were waited for; matrix products, arithmetic and copies ran while one was open for 11% of the time, Pallas kernels for 0%

profile of v1, /device:TPU:0, one launch (start us, length us, event | category | flops | bytes accessed | tf_op | source)
XLA Modules:
  0.0 168.9 jit_solution(2384134481007129503)
XLA Ops:
  9.3 21.9 %all-gather.3.cloned.1.call-done = bf16[384,2048]{1,0:T(8,128)(2,1)} async-done(((bf16[96,2048]{1,0:T(8,128)(2,1)}), bf16[384,2048]{1,0:T(8,128)(2,1)}) %all-gather.3.cloned.1.call-update) | async-done | bytes 1572880 | tf_op jit(solution)/shard_map/all_gather | solution.py:57
  31.3 2.4 %convolution_convert_fusion.3 = bf16[384,256]{1,0:T(8,128)(2,1)S(1)} fusion(bf16[384,2048]{1,0:T(8,128)(2,1)} %all-gather.3.cloned.1.call-done, bf16[2048,256]{1,0:T(8,128)(2,1)} %param.20), kind=kOutput, calls=%fused_computation.32 | convolution fusion | flops 402751488 | bytes 2818048 | tf_op jit(solution)/shard_map/dot_general | solution.py:51
  33.7 1.5 collective-permute-start
  35.8 7.7 %collective-permute-done = bf16[384,256]{1,0:T(8,128)(2,1)S(1)} collective-permute-done((bf16[384,256]{1,0:T(8,128)(2,1)S(1)}, bf16[384,256]{1,0:T(8,128)(2,1)S(1)}, u32[]{:S(2)}, u32[]{:S(2)}) %collective-permute-start) | collective-permute-done | bytes 196640 | tf_op jit(solution)/shard_map/ppermute | solution.py:91
  44.3 8.1 %collective-permute-done.1 = bf16[384,256]{1,0:T(8,128)(2,1)S(1)} collective-permute-done((bf16[384,256]{1,0:T(8,128)(2,1)S(1)}, bf16[384,256]{1,0:T(8,128)(2,1)S(1)}, u32[]{:S(2)}, u32[]{:S(2)}) %collective-permute-start.1) | collective-permute-done | bytes 196640 | tf_op jit(solution)/shard_map/ppermute | solution.py:91
  53.2 1.3 collective-permute-start.7
  54.5 6.2 %collective-permute-done.2 = bf16[384,256]{1,0:T(8,128)(2,1)S(1)} collective-permute-done((bf16[384,256]{1,0:T(8,128)(2,1)S(1)}, bf16[384,256]{1,0:T(8,128)(2,1)S(1)}, u32[]{:S(2)}, u32[]{:S(2)}) %collective-permute-start.2) | collective-permute-done | bytes 196640 | tf_op jit(solution)/shard_map/ppermute | solution.py:91
  60.8 1.4 convolution_convert_fusion.4
  62.2 7.0 %collective-permute-done.3 = bf16[384,256]{1,0:T(8,128)(2,1)} collective-permute-done((bf16[384,256]{1,0:T(8,128)(2,1)S(1)}, bf16[384,256]{1,0:T(8,128)(2,1)}, u32[]{:S(2)}, u32[]{:S(2)}) %collective-permute-start.3) | collective-permute-done | bytes 196640 | tf_op jit(solution)/shard_map/ppermute | solution.py:91
  69.2 1.3 convolution_convert_fusion.5
  70.5 1.8 %copy.22 = bf16[384,2,128]{2,0,1:T(8,128)(2,1)} copy(bf16[384,2,128]{0,2,1:T(8,128)(2,1)} %bitcast.49) | data formatting | bytes 393216
  72.5 5.4 %collective-permute-done.4 = bf16[384,256]{1,0:T(8,128)(2,1)} collective-permute-done((bf16[384,256]{1,0:T(8,128)(2,1)}, bf16[384,256]{1,0:T(8,128)(2,1)}, u32[]{:S(2)}, u32[]{:S(2)}) %collective-permute-start.4) | collective-permute-done | bytes 196640 | tf_op jit(solution)/shard_map/ppermute | solution.py:91
  77.9 2.0 %bitcast_reduce_fusion = (f32[384,2]{0,1:T(2,128)S(1)}, f32[384,256]{0,1:T(8,128)S(1)}) fusion(f32[386,256]{0,1:T(8,128)S(1)} %maximum_convert_fusion, f32[256]{0:T(256)} %bitcast.51, f32[256]{0:T(256)} %bitcast.52, f32[256]{0:T(256)S(1)} %bitcast.50, bf16[384,2048]{1,0:T(8,128)(2,1)S(1)} %copy-done.1, bf16[2048,256]{1,0:T(8,128)(2,1)} %param.21), kind=kOutput, calls=%fused_computation.44 | convolution fusion | flops 403635456 | bytes 4200448 | tf_op jit(solution)/shard_map/dot_general | solution.py:51
  79.9 8.2 %collective-permute-done.5 = bf16[384,256]{1,0:T(8,128)(2,1)S(1)} collective-permute-done((bf16[384,256]{1,0:T(8,128)(2,1)}, bf16[384,256]{1,0:T(8,128)(2,1)S(1)}, u32[]{:S(2)}, u32[]{:S(2)}) %collective-permute-start.5) | collective-permute-done | bytes 196640 | tf_op jit(solution)/shard_map/ppermute | solution.py:91
  88.2 9.3 %collective-permute-done.6 = bf16[384,256]{1,0:T(8,128)(2,1)S(1)} collective-permute-done((bf16[384,256]{1,0:T(8,128)(2,1)S(1)}, bf16[384,256]{1,0:T(8,128)(2,1)S(1)}, u32[]{:S(2)}, u32[]{:S(2)}) %collective-permute-start.6) | collective-permute-done | bytes 196640 | tf_op jit(solution)/shard_map/ppermute | solution.py:91
  101.6 1.6 constant_dynamic-slice_fusion.3
  103.2 1.7 %copy.23 = bf16[3072,256]{0,1:T(8,128)(2,1)S(1)} copy(bf16[3072,256]{1,0:T(8,128)(2,1)} %constant_dynamic-slice_fusion.3) | data formatting | bytes 3145728
  105.0 14.0 %all-gather.5.cloned.1.call-done = bf16[3072,256]{1,0:T(8,128)(2,1)} async-done(((bf16[384,256]{1,0:T(8,128)(2,1)}), bf16[3072,256]{1,0:T(8,128)(2,1)}) %all-gather.5.cloned.1.call-update) | async-done | bytes 1572880 | tf_op jit(solution)/shard_map/all_gather | solution.py:88
  118.9 2.6 %copy.21 = bf16[3072,256]{0,1:T(8,128)(2,1)} copy(bf16[3072,256]{1,0:T(8,128)(2,1)} %all-gather.5.cloned.1.call-done) | data formatting | bytes 3145728
  121.6 5.5 %while.18 = (s32[]{:T(128)}, f32[384,2]{0,1:T(2,128)S(1)}, f32[384,2]{0,1:T(2,128)S(1)}, f32[384,2,128]{0,2,1:T(8,128)S(1)}, s32[]{:T(128)}, /*index=5*/bf16[307...) while((s32[]{:T(128)}, f32[384,2]{0,1:T(2,128)S(1)}, ...), condition=%wide.region_5.6_spmd.clone, body=%wide.region_0.5_spmd.clone.sunk | while | flops 617748864 | bytes 22327704 | solution.py:134
  121.6 5.4 %conditional.3 = ((f32[384,2]{0,1:T(2,128)S(1)}, f32[384,2]{0,1:T(2,128)S(1)}, f32[384,2,128]{0,2,1:T(8,128)S(1)})) conditional(s32[]{:T(128)} %convert_element_type.120, (f32[384,2]{0,1:T(2,128)S(1)}, f32[384,2]{0,1:T(2,128)S(1)}, f32[384,2,128]{0,2,1:T(8,128)S(1)}) %tuple.51, (s32[]{:T(128)}, s32[]{:T(128)}, s32[]{:T(128)}, ...), branch_computations={%region_1.1_spmd, %region_2.4_spmd} | conditional | flops 617748864 | bytes 22325888 | solution.py:132
  123.4 1.5 select_reduce_fusion
  128.5 1.8 %add_convert_fusion = bf16[384,2048]{1,0:T(8,128)(2,1)} fusion(f32[384,2048]{1,0:T(8,128)S(1)} %fusion.28, bf16[384,256]{0,1:T(8,128)(2,1)S(1)} %fusion.26, bf16[256,2048]{1,0:T(8,128)(2,1)S(1)} %copy-done.5), kind=kOutput, calls=%fused_computation.23 | convolution fusion | flops 404226048 | bytes 5963776 | tf_op jit(solution)/shard_map/dot_general | solution.py:141
  130.3 32.0 %reduce-scatter.2.cloned.1.call-done = bf16[96,2048]{1,0:T(8,128)(2,1)} async-done(((bf16[384,2048]{1,0:T(8,128)(2,1)}), bf16[96,2048]{1,0:T(8,128)(2,1)}) %reduce-scatter.2.cloned.1.call-update) | async-done | bytes 393232 | tf_op jit(solution)/shard_map/reduce_scatter | solution.py:138
  (88 shorter events, 14.5 us)
Async XLA Ops:
  6.5 120.9 %copy-start = (bf16[256,2048]{1,0:T(8,128)(2,1)S(1)}, bf16[256,2048]{1,0:T(8,128)(2,1)}, u32[]{:S(2)}) copy-start(bf16[256,2048]{1,0:T(8,128)(2,1)} %param.28) | copy-start | bytes 3145732
  6.5 28.7 %copy-start.12 = (bf16[3,256]{1,0:T(4,128)(2,1)S(1)}, bf16[3,256]{1,0:T(4,128)(2,1)}, u32[]{:S(2)}) copy-start(bf16[3,256]{1,0:T(4,128)(2,1)} %param.24) | copy-start | bytes 4612
  6.5 24.7 %all-gather.3.cloned.1.call-start = ((), (), s32[]{:S(2)}) async-start(), calls=%async_computation.1 | async-start | bytes 1966080 | tf_op jit(solution)/shard_map/all_gather | solution.py:57
  7.3 111.6 %all-gather.5.cloned.1.call-start = ((), (), s32[]{:S(2)}) async-start(), calls=%async_computation.2 | async-start | bytes 1769472 | tf_op jit(solution)/shard_map/all_gather | solution.py:88
  31.3 12.2 %copy-start.1 = (bf16[384,2048]{1,0:T(8,128)(2,1)S(1)}, bf16[384,2048]{1,0:T(8,128)(2,1)}, u32[]{:S(2)}) copy-start(bf16[384,2048]{1,0:T(8,128)(2,1)} %all-gather.3.cloned.1.call-done) | copy-start | bytes 4718596
  31.3 12.2 %copy-start.2 = (bf16[2048,256]{1,0:T(8,128)(2,1)S(1)}, bf16[2048,256]{1,0:T(8,128)(2,1)}, u32[]{:S(2)}) copy-start(bf16[2048,256]{1,0:T(8,128)(2,1)} %param.22) | copy-start | bytes 3145732
  31.3 21.1 %copy-start.3 = (bf16[2048,256]{1,0:T(8,128)(2,1)S(1)}, bf16[2048,256]{1,0:T(8,128)(2,1)}, u32[]{:S(2)}) copy-start(bf16[2048,256]{1,0:T(8,128)(2,1)} %param.23) | copy-start | bytes 3145732
  33.7 9.8 %collective-permute-start = (bf16[384,256]{1,0:T(8,128)(2,1)S(1)}, bf16[384,256]{1,0:T(8,128)(2,1)S(1)}, u32[]{:S(2)}, u32[]{:S(2)}) collective-permute-start(bf16[384,256]{1,0:T(8,128)(2,1)S(1)} %convolution_convert_fusion.3), channel_id=1, source_target_pairs={{0,4},{4,8},{8,12},{12,16},{16,20},{20,24},{24,28},{28,0},{1,5},{5... | collective-permute-start | bytes 589832 | tf_op jit(solution)/shard_map/ppermute | solution.py:91
  35.8 24.9 %copy-start.4 = (bf16[2048,256]{1,0:T(8,128)(2,1)S(1)}, bf16[2048,256]{1,0:T(8,128)(2,1)}, u32[]{:S(2)}) copy-start(bf16[2048,256]{1,0:T(8,128)(2,1)} %param.18) | copy-start | bytes 3145732
  43.5 8.9 %collective-permute-start.1 = (bf16[384,256]{1,0:T(8,128)(2,1)S(1)}, bf16[384,256]{1,0:T(8,128)(2,1)S(1)}, u32[]{:S(2)}, u32[]{:S(2)}) collective-permute-start(bf16[384,256]{1,0:T(8,128)(2,1)S(1)} %collective-permute-done), channel_id=1, source_target_pairs={{0,4},{4,8},{8,12},{12,16},{16,20},{20,24},{24,28},{28,0},{1,5},{5... | collective-permute-start | bytes 589832 | tf_op jit(solution)/shard_map/ppermute | solution.py:91
  44.3 24.9 %copy-start.13 = (bf16[2048,256]{1,0:T(8,128)(2,1)S(1)}, bf16[2048,256]{1,0:T(8,128)(2,1)}, u32[]{:S(2)}) copy-start(bf16[2048,256]{1,0:T(8,128)(2,1)} %param.19) | copy-start | bytes 3145732
  52.4 18.1 %copy-start.6 = (bf16[384,256]{1,0:T(8,128)(2,1)}, bf16[384,256]{1,0:T(8,128)(2,1)S(1)}, u32[]{:S(2)}) copy-start(bf16[384,256]{1,0:T(8,128)(2,1)S(1)} %collective-permute-done.1) | copy-start | bytes 589828
  52.4 8.4 %collective-permute-start.2 = (bf16[384,256]{1,0:T(8,128)(2,1)S(1)}, bf16[384,256]{1,0:T(8,128)(2,1)S(1)}, u32[]{:S(2)}, u32[]{:S(2)}) collective-permute-start(bf16[384,256]{1,0:T(8,128)(2,1)S(1)} %collective-permute-done.1), channel_id=1, source_target_pairs={{0,4},{4,8},{8,12},{12,16},{16,20},{20,24},{24,28},{28,0},{1,5},{5... | collective-permute-start | bytes 589832 | tf_op jit(solution)/shard_map/ppermute | solution.py:91
  53.2 19.1 %collective-permute-start.7 = (bf16[2,256]{0,1:T(8,128)(2,1)S(1)}, bf16[2,256]{0,1:T(8,128)(2,1)S(1)}, u32[]{:S(2)}, u32[]{:S(2)}) collective-permute-start(bf16[2,256]{0,1:T(8,128)(2,1)S(1)} %slice.28), channel_id=1, source_target_pairs={{0,4},{4,8},{8,12},{12,16},{16,20},{20,24},{24,28},{1,5},{5,9},{9,... | collective-permute-start | bytes 3080 | tf_op jit(solution)/shard_map/ppermute | solution.py:13
  60.7 1.5 copy-start.8
  60.7 8.5 %collective-permute-start.3 = (bf16[384,256]{1,0:T(8,128)(2,1)S(1)}, bf16[384,256]{1,0:T(8,128)(2,1)}, u32[]{:S(2)}, u32[]{:S(2)}) collective-permute-start(bf16[384,256]{1,0:T(8,128)(2,1)S(1)} %collective-permute-done.2), channel_id=1, source_target_pairs={{0,4},{4,8},{8,12},{12,16},{16,20},{20,24},{24,28},{28,0},{1,5},{5... | collective-permute-start | bytes 589832 | tf_op jit(solution)/shard_map/ppermute | solution.py:91
  69.2 8.7 %collective-permute-start.4 = (bf16[384,256]{1,0:T(8,128)(2,1)}, bf16[384,256]{1,0:T(8,128)(2,1)}, u32[]{:S(2)}, u32[]{:S(2)}) collective-permute-start(bf16[384,256]{1,0:T(8,128)(2,1)} %collective-permute-done.3), channel_id=1, source_target_pairs={{0,4},{4,8},{8,12},{12,16},{16,20},{20,24},{24,28},{28,0},{1,5},{5... | collective-permute-start | bytes 589832 | tf_op jit(solution)/shard_map/ppermute | solution.py:91
  72.3 90.1 %reduce-scatter.2.cloned.1.call-start = ((), (), s32[]{:S(2)}) async-start(), calls=%async_computation.3 | async-start | bytes 1966080 | tf_op jit(solution)/shard_map/reduce_scatter | solution.py:138
  72.3 27.2 %copy-start.9 = (bf16[384,256]{1,0:T(8,128)(2,1)S(1)}, bf16[384,256]{1,0:T(8,128)(2,1)}, u32[]{:S(2)}) copy-start(bf16[384,256]{1,0:T(8,128)(2,1)} %copy-done.8) | copy-start | bytes 589828
  72.5 27.0 %copy-start.7 = (bf16[384,256]{1,0:T(8,128)(2,1)S(1)}, bf16[384,256]{1,0:T(8,128)(2,1)}, u32[]{:S(2)}) copy-start(bf16[384,256]{1,0:T(8,128)(2,1)} %copy-done.6) | copy-start | bytes 589828
  77.9 10.2 %collective-permute-start.5 = (bf16[384,256]{1,0:T(8,128)(2,1)}, bf16[384,256]{1,0:T(8,128)(2,1)S(1)}, u32[]{:S(2)}, u32[]{:S(2)}) collective-permute-start(bf16[384,256]{1,0:T(8,128)(2,1)} %collective-permute-done.4), channel_id=1, source_target_pairs={{0,4},{4,8},{8,12},{12,16},{16,20},{20,24},{24,28},{28,0},{1,5},{5... | collective-permute-start | bytes 589832 | tf_op jit(solution)/shard_map/ppermute | solution.py:91
  88.1 9.4 %collective-permute-start.6 = (bf16[384,256]{1,0:T(8,128)(2,1)S(1)}, bf16[384,256]{1,0:T(8,128)(2,1)S(1)}, u32[]{:S(2)}, u32[]{:S(2)}) collective-permute-start(bf16[384,256]{1,0:T(8,128)(2,1)S(1)} %collective-permute-done.5), channel_id=1, source_target_pairs={{0,4},{4,8},{8,12},{12,16},{16,20},{20,24},{24,28},{28,0},{1,5},{5... | collective-permute-start | bytes 589832 | tf_op jit(solution)/shard_map/ppermute | solution.py:91
  103.2 18.4 %copy-start.10 = (bf16[384,2,128]{2,0,1:T(8,128)(2,1)S(1)}, bf16[384,2,128]{2,0,1:T(8,128)(2,1)}, u32[]{:S(2)}) copy-start(bf16[384,2,128]{2,0,1:T(8,128)(2,1)} %copy.22) | copy-start | bytes 589828
  103.2 18.4 %copy-start.11 = (f32[2,3072]{1,0:T(2,128)S(1)}, f32[2,3072]{1,0:T(2,128)}, u32[]{:S(2)}) copy-start(f32[2,3072]{1,0:T(2,128)} %param.25) | copy-start | bytes 73732
  (1 other events, 1.2 us)
Sparse Core Ops, SparseCore 0:
  8.9 22.3 all-gather.2
  72.4 46.4 all-gather.4
  130.4 31.8 reduce-scatter.1
